TPU v7x, 32 devices: a whole 2x2x4 slice. The times are simulated.
32 devices in a mesh: sp: 8 (over z, x), tp: 4 (over y, core).
Axes of the slice: x: 2, y: 2, z: 4, core: 2. Of those that a mesh axis runs over, the one named last changes fastest.
Arguments:
- residual: bfloat16 [4096, 2048], P('sp'), may hold values from -6 to 6
- queries: bfloat16 [4096, 1024], P('sp', 'tp'), may hold values from -384 to 384
- key_pairs: bfloat16 [4096, 1024], P('sp', 'tp'), may hold values from -384 to 384
- values: bfloat16 [4096, 1024], P('sp', 'tp'), may hold values from -6 to 6
- lambdas: float32 [8], P('tp'), may hold values from 0.3 to 0.8
- head_gain: float32 [128], replicated, may hold values from 0.1 to 1.9
- w_out: bfloat16 [1024, 2048], replicated, may hold values from -0.1875 to 0.1875
- norm_gain: float32 [2048], replicated, may hold values from 0.1 to 1.9
- w_gate: bfloat16 [2048, 5632], P('sp', 'tp'), may hold values from -0.125 to 0.125
- w_up: bfloat16 [2048, 5632], P('sp', 'tp'), may hold values from -0.125 to 0.125
- w_down: bfloat16 [5632, 2048], P('tp', 'sp'), may hold values from -0.078125 to 0.078125
Outputs:
- layer_out: bfloat16 [4096, 2048], P(('sp', 'tp'))
All inputs are finite; a program needn't handle non-finite values.
Results may differ from a plain program's by a relative error of at most 0.018.
Values may be sent and summed in bfloat16 or wider, within the bound.
A program may use at most 128 MiB of HBM per device.

v0:
```python
import math
import jax
import jax.numpy as jnp
from jax import lax
from jax.sharding import PartitionSpec as P

HD = 64


def per_device(
    residual, queries, key_pairs, values, lambdas, head_gain, w_out, norm_gain, w_gate, w_up, w_down
):
    local_rows = queries.shape[0]
    heads_here = lambdas.shape[0]
    value_width = values.shape[1] // heads_here
    score_scale = HD ** (-0.5)
    query_view = queries.reshape(local_rows, heads_here, 2, HD)

    def update(carry, key_block, value_block):
        highest, totals, mixture = carry
        scores = (
            jnp.einsum("qhmd,khmd->hmqk", query_view, key_block, preferred_element_type=jnp.float32)
            * score_scale
        )
        new_high = jnp.maximum(highest, jnp.max(scores, axis=-1))
        shrink = jnp.exp(highest - new_high)
        weights = jnp.exp(scores - new_high[..., None])
        totals = totals * shrink + jnp.sum(weights, axis=-1)
        mixture = mixture * shrink[..., None] + jnp.einsum(
            "hmqk,khe->hmqe",
            weights.astype(jnp.bfloat16),
            value_block,
            preferred_element_type=jnp.float32,
        )
        return (new_high, totals, mixture)

    initial = (
        jnp.full((heads_here, 2, local_rows), -jnp.inf, jnp.float32),
        jnp.zeros((heads_here, 2, local_rows), jnp.float32),
        jnp.zeros((heads_here, 2, local_rows, value_width), jnp.float32),
    )
    key_piece = lax.all_gather(key_pairs, "sp", axis=0, tiled=True)
    value_piece = lax.all_gather(values, "sp", axis=0, tiled=True)
    length = key_piece.shape[0]
    span = math.gcd(length, 512)
    key_blocks = key_piece.reshape(length // span, span, heads_here, 2, HD)
    value_blocks = value_piece.reshape(length // span, span, heads_here, value_width)

    def advance(position, inner):
        return update(inner, key_blocks[position], value_blocks[position])

    highest, totals, mixture = lax.fori_loop(0, length // span, advance, initial)
    mixed = mixture / totals[..., None]
    differ = mixed[:, 0] - lambdas[:, None, None] * mixed[:, 1]
    normed_heads = (
        differ * lax.rsqrt(jnp.mean(differ * differ, axis=-1, keepdims=True) + 1e-05) * head_gain
    )
    heads_out = (
        jnp.transpose(normed_heads, (1, 0, 2))
        .reshape(local_rows, heads_here * value_width)
        .astype(jnp.bfloat16)
    )
    tp_index = lax.axis_index("tp")
    own_rows = local_rows // lax.axis_size("tp")
    own_begin = tp_index * own_rows
    w_mine = lax.dynamic_slice_in_dim(
        w_out, tp_index * heads_here * value_width, heads_here * value_width, 0
    )
    projected = lax.psum_scatter(
        jnp.dot(heads_out, w_mine, preferred_element_type=jnp.float32).astype(jnp.bfloat16),
        "tp",
        scatter_dimension=0,
        tiled=True,
    ).astype(jnp.float32)
    residual_own = lax.dynamic_slice_in_dim(residual, own_begin, own_rows, 0)
    hidden_own = (residual_own.astype(jnp.float32) + projected).astype(jnp.bfloat16)
    stream_f = hidden_own.astype(jnp.float32)
    scaled = stream_f * lax.rsqrt(jnp.mean(stream_f * stream_f, axis=-1, keepdims=True) + 1e-05)
    normed_rows = lax.all_gather(
        (scaled * norm_gain).astype(jnp.bfloat16), "tp", axis=0, tiled=True
    )
    unit_width = w_gate.shape[1]
    joined = jnp.concatenate([w_gate, w_up], axis=1)
    both_sums = jnp.dot(
        normed_rows,
        lax.all_gather(joined, "sp", axis=0, tiled=True),
        preferred_element_type=jnp.float32,
    )
    gate_sum = both_sums[:, :unit_width]
    up_sum = both_sums[:, unit_width:]
    hidden_units = (jax.nn.silu(gate_sum) * up_sum).astype(jnp.bfloat16)
    down_whole = lax.all_gather(w_down, "sp", axis=1, tiled=True)
    ffn_out = lax.psum_scatter(
        jnp.dot(hidden_units, down_whole, preferred_element_type=jnp.float32).astype(jnp.bfloat16),
        "tp",
        scatter_dimension=0,
        tiled=True,
    ).astype(jnp.float32)
    return (hidden_own.astype(jnp.float32) + ffn_out).astype(jnp.bfloat16)


def solution(mesh):
    placed = (
        P("sp", None),
        P("sp", "tp"),
        P("sp", "tp"),
        P("sp", "tp"),
        P("tp"),
        P(),
        P(),
        P(),
        P("sp", "tp"),
        P("sp", "tp"),
        P("tp", "sp"),
    )
    return jax.shard_map(
        per_device, mesh=mesh, in_specs=placed, out_specs=P(("sp", "tp"), None), check_vma=False
    )
```

profile of v0, /device:TPU:0, one launch (start us, length us, event | category | flops | bytes accessed | tf_op | source)
XLA Modules:
  0.0 547.7 jit_solution(14696506700024109413)
XLA Ops:
  6.5 0.7 all-gather.6.cloned.1.call-update
  7.3 0.7 all-gather.8.cloned.1.call-update
  8.0 0.0 reduce-scatter.3.cloned.1.call-start
  8.1 1.1 copy.17
  9.2 52.1 %all-gather.6.cloned.1.call-done = bf16[4096,256]{1,0:T(8,128)(2,1)} async-done(((bf16[512,256]{1,0:T(8,128)(2,1)}), bf16[4096,256]{1,0:T(8,128)(2,1)}) %all-gather.6.cloned.1.call-update) | async-done | bytes 2097168 | tf_op jit(solution)/shard_map/all_gather | solution.py:42
  61.3 8.3 %reshape.37 = bf16[8,512,2,2,64]{4,3,2,1,0:T(2,128)(2,1)} reshape(bf16[4096,256]{1,0:T(8,128)(2,1)} %all-gather.6.cloned.1.call-done) | data formatting | bytes 4194304 | tf_op jit(solution)/shard_map/reshape | solution.py:46
  69.6 9.1 %copy.19 = bf16[8,512,2,2,64]{1,4,3,2,0:T(8,128)(2,1)S(1)} copy(bf16[8,512,2,2,64]{4,3,2,1,0:T(2,128)(2,1)} %reshape.37) | data formatting | bytes 4194304
  78.7 32.4 %all-gather.8.cloned.1.call-done = bf16[4096,256]{1,0:T(8,128)(2,1)} async-done(((bf16[512,256]{1,0:T(8,128)(2,1)}), bf16[4096,256]{1,0:T(8,128)(2,1)}) %all-gather.8.cloned.1.call-update) | async-done | bytes 2097168 | tf_op jit(solution)/shard_map/all_gather | solution.py:43
  111.1 4.0 reshape.38
  115.0 67.2 %while.18 = (s32[]{:T(128)}, f32[2,2,512]{2,1,0:T(2,128)S(1)}, f32[2,2,512]{2,1,0:T(2,128)S(1)}, f32[2,2,512,128]{3,2,1,0:T(8,128)S(1)}, bf16[8,512,2,2,64]{1,4,...) while((s32[]{:T(128)}, f32[2,2,512]{2,1,0:T(2,128)S(1)}, ...), condition=%wide.region_3.0_spmd.clone, body=%wide.region_0.0_spmd.clone.sunk | while | flops 411838464 | bytes 32899212 | solution.py:52
  115.0 2.7 bitcast_reduce_fusion.2
  117.7 3.0 fusion.44
  120.8 1.1 constant_dynamic-slice_fusion.2
  122.0 1.4 fusion.46
  123.4 2.7 bitcast_reduce_fusion.2
  126.1 3.0 fusion.44
  129.2 1.1 constant_dynamic-slice_fusion.2
  130.4 1.4 fusion.46
  131.8 2.7 bitcast_reduce_fusion.2
  134.5 3.0 fusion.44
  137.6 1.1 constant_dynamic-slice_fusion.2
  138.8 1.4 fusion.46
  140.2 2.7 bitcast_reduce_fusion.2
  142.9 3.0 fusion.44
  146.0 1.1 constant_dynamic-slice_fusion.2
  147.2 1.4 fusion.46
  148.6 2.7 bitcast_reduce_fusion.2
  151.3 3.0 fusion.44
  154.4 1.1 constant_dynamic-slice_fusion.2
  155.6 1.4 fusion.46
  157.0 2.7 bitcast_reduce_fusion.2
  159.7 3.0 fusion.44
  162.8 1.1 constant_dynamic-slice_fusion.2
  164.0 1.4 fusion.46
  165.4 2.7 bitcast_reduce_fusion.2
  168.1 3.0 fusion.44
  171.2 1.1 constant_dynamic-slice_fusion.2
  172.4 1.4 fusion.46
  173.8 2.7 bitcast_reduce_fusion.2
  176.5 3.0 fusion.44
  179.6 1.1 constant_dynamic-slice_fusion.2
  180.8 1.4 fusion.46
  182.2 0.3 copy.22
  182.6 0.2 broadcast_divide_fusion
  182.7 0.1 copy-done.4
  182.9 0.2 multiply_reduce_fusion
  183.1 0.1 multiply_convert_fusion
  183.2 3.3 convolution_convert_fusion
  186.6 0.0 all-gather.10.cloned.1.call-start
  186.6 29.8 %reduce-scatter.3.cloned.1.call-done = bf16[128,2048]{1,0:T(8,128)(2,1)} async-done(((bf16[512,2048]{1,0:T(8,128)(2,1)}), bf16[128,2048]{1,0:T(8,128)(2,1)}) %reduce-scatter.3.cloned.1.call-update) | async-done | bytes 524304 | tf_op jit(solution)/shard_map/reduce_scatter | solution.py:69
  216.4 1.5 fusion.20
  217.9 1.0 fusion.22
  218.9 0.0 all-gather.12.cloned.1.call-start
  219.0 1.2 pad_maximum_fusion
  220.2 0.0 all-gather.14.cloned.1.call-start
  220.3 0.5 all-gather.14.cloned.1.call-update
  220.8 0.2 reduce-scatter.5.cloned.1.call-start
  221.0 20.6 %all-gather.10.cloned.1.call-done = bf16[512,2048]{1,0:T(8,128)(2,1)} async-done(((bf16[128,2048]{1,0:T(8,128)(2,1)}), bf16[512,2048]{1,0:T(8,128)(2,1)}) %all-gather.10.cloned.1.call-update) | async-done | bytes 2097168 | tf_op jit(solution)/shard_map/all_gather | solution.py:79
  241.6 165.4 %all-gather.12.cloned.1.call-done = bf16[2048,2816]{1,0:T(8,128)(2,1)} async-done(((bf16[256,2816]{1,0:T(8,128)(2,1)}), bf16[2048,2816]{1,0:T(8,128)(2,1)}) %all-gather.12.cloned.1.call-update) | async-done | bytes 11534352 | tf_op jit(solution)/shard_map/all_gather | solution.py:86
  407.0 12.5 %fusion.29 = f32[512,2816]{1,0:T(8,128)} fusion(bf16[512,2048]{1,0:T(8,128)(2,1)} %all-gather.10.cloned.1.call-done, bf16[2048,2816]{1,0:T(8,128)(2,1)} %all-gather.12.cloned.1.call-done), kind=kOutput, calls=%fused_computation.48 | convolution fusion | flops 5905580032 | bytes 19398656 | tf_op jit(solution)/shard_map/dot_general | solution.py:84
  419.5 80.7 %all-gather.14.cloned.1.call-done = bf16[1408,2048]{1,0:T(8,128)(2,1)} async-done(((bf16[1408,256]{1,0:T(8,128)(2,1)}), bf16[1408,2048]{1,0:T(8,128)(2,1)}) %all-gather.14.cloned.1.call-update) | async-done | bytes 5767184 | tf_op jit(solution)/shard_map/all_gather | solution.py:92
  500.2 9.1 %convolution_convert_fusion.1 = bf16[512,2048]{1,0:T(8,128)(2,1)} fusion(bf16[1408,2048]{1,0:T(8,128)(2,1)} %all-gather.14.cloned.1.call-done, f32[512,2816]{1,0:T(8,128)} %fusion.29), kind=kOutput, calls=%fused_computation.23 | convolution fusion | flops 2958163968 | bytes 13631488 | tf_op jit(solution)/shard_map/dot_general | solution.py:94
  509.4 29.5 %reduce-scatter.5.cloned.1.call-done = bf16[128,2048]{1,0:T(8,128)(2,1)} async-done(((bf16[512,2048]{1,0:T(8,128)(2,1)}), bf16[128,2048]{1,0:T(8,128)(2,1)}) %reduce-scatter.5.cloned.1.call-update) | async-done | bytes 524304 | tf_op jit(solution)/shard_map/reduce_scatter | solution.py:93
  538.9 2.0 fusion.23
  (61 shorter events, 0.5 us)
Async XLA Ops:
  6.5 54.8 %all-gather.6.cloned.1.call-start = ((), (), s32[]{:S(2)}) async-start(), calls=%async_computation.2 | async-start | bytes 2359296 | tf_op jit(solution)/shard_map/all_gather | solution.py:42
  7.3 103.8 %all-gather.8.cloned.1.call-start = ((), (), s32[]{:S(2)}) async-start(), calls=%async_computation.3 | async-start | bytes 2359296 | tf_op jit(solution)/shard_map/all_gather | solution.py:43
  8.0 208.4 %reduce-scatter.3.cloned.1.call-start = ((), (), s32[]{:S(2)}) async-start(), calls=%async_computation.4 | async-start | bytes 2621440 | tf_op jit(solution)/shard_map/reduce_scatter | solution.py:69
  117.7 4.2 copy-start
  126.1 4.2 copy-start
  134.5 4.2 copy-start
  142.9 4.2 copy-start
  151.3 4.2 copy-start
  159.7 4.2 copy-start
  168.1 4.2 copy-start
  176.5 4.2 copy-start
  182.2 0.7 copy-start.4
  182.2 0.8 copy-start.5
  186.5 31.4 %copy-start.3 = (f32[2048]{0:T(1024)S(1)}, f32[2048]{0:T(1024)}, u32[]{:S(2)}) copy-start(f32[2048]{0:T(1024)} %param.20) | copy-start | bytes 24580
  186.5 32.4 %copy-start.1 = (bf16[256,1408]{1,0:T(8,128)(2,1)S(1)}, bf16[256,1408]{1,0:T(8,128)(2,1)}, u32[]{:S(2)}) copy-start(bf16[256,1408]{1,0:T(8,128)(2,1)} %param.22) | copy-start | bytes 2162692
  186.5 32.4 %copy-start.2 = (bf16[256,1408]{1,0:T(8,128)(2,1)S(1)}, bf16[256,1408]{1,0:T(8,128)(2,1)}, u32[]{:S(2)}) copy-start(bf16[256,1408]{1,0:T(8,128)(2,1)} %param.21) | copy-start | bytes 2162692
  186.6 55.1 %all-gather.10.cloned.1.call-start = ((), (), s32[]{:S(2)}) async-start(), calls=%async_computation.5 | async-start | bytes 2621440 | tf_op jit(solution)/shard_map/all_gather | solution.py:79
  218.9 188.1 %all-gather.12.cloned.1.call-start = ((), (), s32[]{:S(2)}) async-start(), calls=%async_computation.6 | async-start | bytes 12976128 | tf_op jit(solution)/shard_map/all_gather | solution.py:86
  220.2 280.0 %all-gather.14.cloned.1.call-start = ((), (), s32[]{:S(2)}) async-start(), calls=%async_computation.7 | async-start | bytes 6488064 | tf_op jit(solution)/shard_map/all_gather | solution.py:92
  220.8 318.1 %reduce-scatter.5.cloned.1.call-start = ((), (), s32[]{:S(2)}) async-start(), calls=%async_computation.8 | async-start | bytes 2621440 | tf_op jit(solution)/shard_map/reduce_scatter | solution.py:93
Sparse Core Ops, SparseCore 0:
  9.5 51.7 all-gather.5
  63.4 47.6 all-gather.7
  186.7 29.6 reduce-scatter.2
  219.0 22.5 all-gather.9
  243.7 163.2 all-gather.11
  408.9 91.2 all-gather.13
  509.5 29.3 reduce-scatter.4
where the time goes:
time: 548 us
  waiting for transfers between devices  412 us (75%)
  matrix products  57.9 us (11%)
  local copies, waits for them, and re-layouts  32.1 us (6%)
  other arithmetic  30.8 us (6%)
  between operations  13.6 us (2%)
    all_gather x1, waiting for transfers between devices, per_device(): lax.all_gather(joined, 'sp', axis=0, tiled=True)  165 us
    all_gather x1, waiting for transfers between devices, per_device(): down_whole = lax.all_gather(w_down, 'sp', axis=1, tiled=True)  80.7 us
    all_gather x1, waiting for transfers between devices, per_device(): key_piece = lax.all_gather(key_pairs, 'sp', axis=0, tiled=True)  52.1 us
    all_gather x1, waiting for transfers between devices, per_device(): value_piece = lax.all_gather(values, 'sp', axis=0, tiled=True)  32.4 us
    reduce_scatter x1, waiting for transfers between devices, per_device(): lax.psum_scatter(jnp.dot(heads_out, w_mine, preferred_element_type=jnp.fl...  29.8 us
    reduce_scatter x1, waiting for transfers between devices, per_device(): lax.psum_scatter(jnp.dot(hidden_units, down_whole, preferred_element_type...  29.5 us
    reduce_sum x8, other arithmetic, update(): totals = totals * shrink + jnp.sum(weights, axis=-1)  24.3 us
    dot_general x8, matrix products, update(): jnp.einsum('qhmd,khmd->hmqk', query_view, key_block, preferred_element_ty...  21.7 us
  transfers between devices with their start and end apart: 7, of which 7 were waited for; matrix products, arithmetic and copies ran while one was open for 6% of the time, Pallas kernels for 0%

commit v1 on v0

--- a/solution.py
+++ b/solution.py
@@ -39,8 +39,9 @@
         jnp.zeros((heads_here, 2, local_rows), jnp.float32),
         jnp.zeros((heads_here, 2, local_rows, value_width), jnp.float32),
     )
-    key_piece = lax.all_gather(key_pairs, "sp", axis=0, tiled=True)
-    value_piece = lax.all_gather(values, "sp", axis=0, tiled=True)
+    top = jnp.concatenate([key_pairs, values], 1)
+    v_next = lax.all_gather(top, "sp", axis=0, tiled=True)
+    key_piece, value_piece = jnp.split(v_next, [key_pairs.shape[1]], 1)
     length = key_piece.shape[0]
     span = math.gcd(length, 512)
     key_blocks = key_piece.reshape(length // span, span, heads_here, 2, HD)

time: 548 us -> 546 us (level)
  waiting for transfers between devices: 412 us -> 402 us
  matrix products: 57.9 us -> 65.5 us
    all_gather x2 -> x1, waiting for transfers between devices: 84.5 us -> 75.4 us  [per_device(): v_next = lax.all_gather(top, 'sp', axis=0, tiled=True)]
    dot_general x8, matrix products: 21.7 us -> 29.3 us  [update(): jnp.einsum('qhmd,khmd->hmqk', query_view, key_block, preferred_element_ty...]
    unnamed x12 -> x14, local copies, waits for them, and re-layouts: 10.3 us -> 12 us
  transfers between devices with their start and end apart: 7 -> 6, of which waited for: 7 -> 6; matrix products, arithmetic and copies ran while one was open for 6% -> 3% of each run, Pallas kernels for 0% -> 0%
where the time goes in v1:
time: 546 us; the launch traced here: 545 us
  waiting for transfers between devices  402 us (74%)
  matrix products  65.5 us (12%)
  other arithmetic  32.6 us (6%)
  local copies, waits for them, and re-layouts  30.6 us (6%)
  between operations  13.6 us (2%)
    all_gather x1, waiting for transfers between devices, per_device(): lax.all_gather(joined, 'sp', axis=0, tiled=True)  165 us
    all_gather x1, waiting for transfers between devices, per_device(): down_whole = lax.all_gather(w_down, 'sp', axis=1, tiled=True)  80.7 us
    all_gather x1, waiting for transfers between devices, per_device(): v_next = lax.all_gather(top, 'sp', axis=0, tiled=True)  75.4 us
    reduce_scatter x1, waiting for transfers between devices, per_device(): lax.psum_scatter(jnp.dot(heads_out, w_mine, preferred_element_type=jnp.fl...  29.8 us
    reduce_scatter x1, waiting for transfers between devices, per_device(): lax.psum_scatter(jnp.dot(hidden_units, down_whole, preferred_element_type...  29.5 us
    dot_general x8, matrix products, update(): jnp.einsum('qhmd,khmd->hmqk', query_view, key_block, preferred_element_ty...  29.3 us
    reduce_sum x8, other arithmetic, update(): totals = totals * shrink + jnp.sum(weights, axis=-1)  24.3 us
    all_gather x1, waiting for transfers between devices, per_device(): lax.all_gather((scaled * norm_gain).astype(jnp.bfloat16), 'tp', axis=0, t...  20.8 us
  transfers between devices with their start and end apart: 6, of which 6 were waited for; matrix products, arithmetic and copies ran while one was open for 3% of the time, Pallas kernels for 0%

profile of v1, /device:TPU:0, one launch (start us, length us, event | category | flops | bytes accessed | tf_op | source)
XLA Modules:
  0.0 545.2 jit_solution(14329110708552235107)
XLA Ops:
  6.5 1.9 pad_maximum_fusion.1
  8.4 0.0 reduce-scatter.3.cloned.1.call-start
  8.5 1.1 copy.17
  9.6 75.4 %all-gather.5.cloned.1.call-done = bf16[4096,512]{1,0:T(8,128)(2,1)} async-done(((bf16[512,512]{1,0:T(8,128)(2,1)}), bf16[4096,512]{1,0:T(8,128)(2,1)}) %all-gather.5.cloned.1.call-update) | async-done | bytes 4194320 | tf_op jit(solution)/shard_map/all_gather | solution.py:43
  85.0 3.8 fusion.29
  88.8 3.2 reshape.37
  92.1 10.7 %copy.19 = bf16[8,512,2,2,64]{1,4,3,2,0:T(8,128)(2,1)} copy(bf16[8,512,2,2,64]{4,3,2,1,0:T(2,128)(2,1)} %reshape.37) | data formatting | bytes 4194304
  102.8 2.1 reshape.38
  104.9 74.7 %while.18 = (s32[]{:T(128)}, f32[2,2,512]{2,1,0:T(2,128)S(1)}, f32[2,2,512]{2,1,0:T(2,128)S(1)}, f32[2,2,512,128]{3,2,1,0:T(8,128)S(1)}, bf16[8,512,2,2,64]{1,4,...) while((s32[]{:T(128)}, f32[2,2,512]{2,1,0:T(2,128)S(1)}, ...), condition=%wide.region_3.0_spmd.clone, body=%wide.region_0.0_spmd.clone.sunk | while | flops 411838464 | bytes 32899720 | solution.py:53
  104.9 3.7 bitcast_reduce_fusion.2
  108.6 3.0 fusion.45
  111.6 1.1 constant_dynamic-slice_fusion.2
  112.8 1.4 fusion.47
  114.2 3.7 bitcast_reduce_fusion.2
  117.9 3.0 fusion.45
  121.0 1.1 constant_dynamic-slice_fusion.2
  122.1 1.4 fusion.47
  123.6 3.7 bitcast_reduce_fusion.2
  127.2 3.0 fusion.45
  130.3 1.1 constant_dynamic-slice_fusion.2
  131.5 1.4 fusion.47
  132.9 3.7 bitcast_reduce_fusion.2
  136.6 3.0 fusion.45
  139.7 1.1 constant_dynamic-slice_fusion.2
  140.8 1.4 fusion.47
  142.2 3.7 bitcast_reduce_fusion.2
  145.9 3.0 fusion.45
  149.0 1.1 constant_dynamic-slice_fusion.2
  150.2 1.4 fusion.47
  151.6 3.7 bitcast_reduce_fusion.2
  155.3 3.0 fusion.45
  158.3 1.1 constant_dynamic-slice_fusion.2
  159.5 1.4 fusion.47
  160.9 3.7 bitcast_reduce_fusion.2
  164.6 3.0 fusion.45
  167.7 1.1 constant_dynamic-slice_fusion.2
  168.8 1.4 fusion.47
  170.3 3.7 bitcast_reduce_fusion.2
  174.0 3.0 fusion.45
  177.0 1.1 constant_dynamic-slice_fusion.2
  178.2 1.4 fusion.47
  179.6 0.3 copy.22
  180.0 0.2 broadcast_divide_fusion
  180.2 0.1 copy-done.5
  180.3 0.2 multiply_reduce_fusion
  180.5 0.1 multiply_convert_fusion
  180.6 3.3 convolution_convert_fusion
  183.9 0.0 reduce-scatter.3.cloned.1.call-update
  184.0 0.0 all-gather.7.cloned.1.call-start
  184.0 29.8 %reduce-scatter.3.cloned.1.call-done = bf16[128,2048]{1,0:T(8,128)(2,1)} async-done(((bf16[512,2048]{1,0:T(8,128)(2,1)}), bf16[128,2048]{1,0:T(8,128)(2,1)}) %reduce-scatter.3.cloned.1.call-update) | async-done | bytes 524304 | tf_op jit(solution)/shard_map/reduce_scatter | solution.py:70
  213.9 1.5 fusion.20
  215.3 1.0 fusion.22
  216.3 0.0 all-gather.9.cloned.1.call-start
  216.4 1.2 pad_maximum_fusion
  217.7 0.0 all-gather.11.cloned.1.call-start
  217.7 0.5 all-gather.11.cloned.1.call-update
  218.3 0.0 reduce-scatter.5.cloned.1.call-start
  218.3 20.8 %all-gather.7.cloned.1.call-done = bf16[512,2048]{1,0:T(8,128)(2,1)} async-done(((bf16[128,2048]{1,0:T(8,128)(2,1)}), bf16[512,2048]{1,0:T(8,128)(2,1)}) %all-gather.7.cloned.1.call-update) | async-done | bytes 2097168 | tf_op jit(solution)/shard_map/all_gather | solution.py:80
  239.1 165.4 %all-gather.9.cloned.1.call-done = bf16[2048,2816]{1,0:T(8,128)(2,1)} async-done(((bf16[256,2816]{1,0:T(8,128)(2,1)}), bf16[2048,2816]{1,0:T(8,128)(2,1)}) %all-gather.9.cloned.1.call-update) | async-done | bytes 11534352 | tf_op jit(solution)/shard_map/all_gather | solution.py:87
  404.4 12.5 %fusion.30 = f32[512,2816]{1,0:T(8,128)} fusion(bf16[512,2048]{1,0:T(8,128)(2,1)} %all-gather.7.cloned.1.call-done, bf16[2048,2816]{1,0:T(8,128)(2,1)} %all-gather.9.cloned.1.call-done), kind=kOutput, calls=%fused_computation.50 | convolution fusion | flops 5905580032 | bytes 19398656 | tf_op jit(solution)/shard_map/dot_general | solution.py:85
  417.0 80.7 %all-gather.11.cloned.1.call-done = bf16[1408,2048]{1,0:T(8,128)(2,1)} async-done(((bf16[1408,256]{1,0:T(8,128)(2,1)}), bf16[1408,2048]{1,0:T(8,128)(2,1)}) %all-gather.11.cloned.1.call-update) | async-done | bytes 5767184 | tf_op jit(solution)/shard_map/all_gather | solution.py:93
  497.7 9.1 %convolution_convert_fusion.1 = bf16[512,2048]{1,0:T(8,128)(2,1)} fusion(bf16[1408,2048]{1,0:T(8,128)(2,1)} %all-gather.11.cloned.1.call-done, f32[512,2816]{1,0:T(8,128)} %fusion.30), kind=kOutput, calls=%fused_computation.23 | convolution fusion | flops 2958163968 | bytes 13631488 | tf_op jit(solution)/shard_map/dot_general | solution.py:95
  506.8 29.5 %reduce-scatter.5.cloned.1.call-done = bf16[128,2048]{1,0:T(8,128)(2,1)} async-done(((bf16[512,2048]{1,0:T(8,128)(2,1)}), bf16[128,2048]{1,0:T(8,128)(2,1)}) %reduce-scatter.5.cloned.1.call-update) | async-done | bytes 524304 | tf_op jit(solution)/shard_map/reduce_scatter | solution.py:94
  536.4 2.0 fusion.23
  (62 shorter events, 0.4 us)
Async XLA Ops:
  6.5 78.5 %all-gather.5.cloned.1.call-start = ((), (), s32[]{:S(2)}) async-start(), calls=%async_computation.2 | async-start | bytes 4718592 | tf_op jit(solution)/shard_map/all_gather | solution.py:43
  8.4 205.4 %reduce-scatter.3.cloned.1.call-start = ((), (), s32[]{:S(2)}) async-start(), calls=%async_computation.3 | async-start | bytes 2621440 | tf_op jit(solution)/shard_map/reduce_scatter | solution.py:70
  92.1 10.7 %copy-start.1 = (bf16[4096,256]{1,0:T(8,128)(2,1)S(1)}, bf16[4096,256]{1,0:T(8,128)(2,1)}, u32[]{:S(2)}) copy-start(bf16[4096,256]{1,0:T(8,128)(2,1)} %get-tuple-element.183) | copy-start | bytes 6291460
  108.5 4.2 copy-start
  117.9 4.2 copy-start
  127.2 4.2 copy-start
  136.6 4.2 copy-start
  145.9 4.2 copy-start
  155.3 4.2 copy-start
  164.6 4.2 copy-start
  173.9 4.2 copy-start
  179.6 0.7 copy-start.5
  179.6 0.8 copy-start.6
  183.9 31.4 %copy-start.4 = (f32[2048]{0:T(1024)S(1)}, f32[2048]{0:T(1024)}, u32[]{:S(2)}) copy-start(f32[2048]{0:T(1024)} %param.20) | copy-start | bytes 24580
  183.9 32.5 %copy-start.2 = (bf16[256,1408]{1,0:T(8,128)(2,1)S(1)}, bf16[256,1408]{1,0:T(8,128)(2,1)}, u32[]{:S(2)}) copy-start(bf16[256,1408]{1,0:T(8,128)(2,1)} %param.22) | copy-start | bytes 2162692
  183.9 32.5 %copy-start.3 = (bf16[256,1408]{1,0:T(8,128)(2,1)S(1)}, bf16[256,1408]{1,0:T(8,128)(2,1)}, u32[]{:S(2)}) copy-start(bf16[256,1408]{1,0:T(8,128)(2,1)} %param.21) | copy-start | bytes 2162692
  184.0 55.1 %all-gather.7.cloned.1.call-start = ((), (), s32[]{:S(2)}) async-start(), calls=%async_computation.4 | async-start | bytes 2621440 | tf_op jit(solution)/shard_map/all_gather | solution.py:80
  216.3 188.1 %all-gather.9.cloned.1.call-start = ((), (), s32[]{:S(2)}) async-start(), calls=%async_computation.5 | async-start | bytes 12976128 | tf_op jit(solution)/shard_map/all_gather | solution.py:87
  217.7 280.0 %all-gather.11.cloned.1.call-start = ((), (), s32[]{:S(2)}) async-start(), calls=%async_computation.6 | async-start | bytes 6488064 | tf_op jit(solution)/shard_map/all_gather | solution.py:93
  218.3 318.1 %reduce-scatter.5.cloned.1.call-start = ((), (), s32[]{:S(2)}) async-start(), calls=%async_computation.7 | async-start | bytes 2621440 | tf_op jit(solution)/shard_map/reduce_scatter | solution.py:94
Sparse Core Ops, SparseCore 0:
  9.5 75.4 all-gather.4
  184.1 29.7 reduce-scatter.2
  216.5 22.5 all-gather.6
  241.1 163.2 all-gather.8
  406.3 91.2 all-gather.10
  507.0 29.3 reduce-scatter.4
